TPU v7x, 32 devices: a whole 2x2x4 slice. The times are simulated.
32 devices in a mesh: grp: 2 (over y), sp: 4 (over z), fs: 2 (over x), tp: 2 (over core).
Axes of the slice: x: 2, y: 2, z: 4, core: 2. Of those that a mesh axis runs over, the one named last changes fastest.
Arguments:
- tokens: bfloat16 [4, 512, 2048], P(('grp', 'fs'), 'sp', 'tp'), parts along dimension 0, may hold values from -120 to 120
- mix_gain: float32 [2048], replicated, may hold values from 0.1 to 1.9
- attn_query: bfloat16 [2048, 1024], P('fs', 'tp'), may hold values from -0.375 to 0.375
- attn_key: bfloat16 [2048, 1024], P('fs', 'tp'), may hold values from -0.125 to 0.125
- attn_value: bfloat16 [2048, 1024], P('fs', 'tp'), may hold values from -0.125 to 0.125
- rec_query: bfloat16 [2048, 1024], P('fs', 'tp'), may hold values from -0.125 to 0.125
- rec_forget: bfloat16 [2048, 1024], P('fs', 'tp'), may hold values from -0.125 to 0.125
- rec_input: bfloat16 [2048, 1024], P('fs', 'tp'), may hold values from -0.125 to 0.125
- break_offset: float32 [8], P('tp'), may hold values from -13.5 to -7
- forget_room: float32 [8, 128], P('tp'), may hold values from 0.0009765625 to 0.05
- out_gain: float32 [128], replicated, may hold values from 0.1 to 1.9
- out_attn: bfloat16 [1024, 2048], P('tp', 'fs'), may hold values from -0.125 to 0.125
- out_rec: bfloat16 [1024, 2048], P('tp', 'fs'), may hold values from -0.125 to 0.125
Outputs:
- mixed: bfloat16 [4, 512, 2048], P(('grp', 'fs'), ('sp', 'tp')), parts along dimension 0
There are 2 independent parts, one for each index of `grp`. A program takes and returns all parts, laid end to end along the dimension named above; an argument that names none is the same for every part. Nothing has to cross between parts.
All inputs are finite; a program needn't handle non-finite values.
Results may differ from a plain program's by a relative error of at most 0.019.
Values may be sent and summed in bfloat16 or wider, within the bound.
A program may use at most 64 MiB of HBM per device.

v0:
```python
import math
import jax
import jax.numpy as jnp
from jax import lax
from jax.sharding import PartitionSpec as P

HEAD = 128
DK = 128
DV = 128
REC_BLOCK = 64
norm_eps = 1e-06
highest = lax.Precision.HIGHEST


def carried_in(x, axis, join, neutral):
    place = lax.axis_index(axis)
    gathered = jax.tree.map(
        lambda a, kind: lax.all_gather(a.astype(kind), axis), x, (jnp.bfloat16, jnp.bfloat16)
    )
    state = jax.tree.map(lambda a, e: jnp.zeros_like(a) + jnp.asarray(e, a.dtype), x, neutral)

    def one(step, state):
        return join(
            state,
            jax.tree.map(
                lambda a, own: lax.dynamic_index_in_dim(a, step, 0, False).astype(own.dtype),
                gathered,
                x,
            ),
        )

    return lax.fori_loop(0, place, one, state)


def block_step(states, inputs):
    queries, key_in, value_rows, log_forget = inputs
    block_len = queries.shape[-2]
    cum_log = jnp.cumsum(log_forget, axis=-2)
    last_log = cum_log[..., -1:, :]
    q_dec = queries * jnp.exp(cum_log)
    k_inv = key_in * jnp.exp(-cum_log)
    causal = lax.iota(jnp.int32, block_len)[:, None] >= lax.iota(jnp.int32, block_len)[None, :]
    carried_part = jnp.einsum("...tk,...kv->...tv", q_dec, states, precision=highest)
    scores = jnp.where(
        causal, jnp.einsum("...tk,...sk->...ts", q_dec, k_inv, precision=highest), 0.0
    )
    inner_part = jnp.einsum("...ts,...sv->...tv", scores, value_rows, precision=highest)
    fresh_state = jnp.einsum(
        "...sk,...sv->...kv", key_in * jnp.exp(last_log - cum_log), value_rows, precision=highest
    )
    return (
        jnp.exp(jnp.swapaxes(last_log, -1, -2)) * states + fresh_state,
        carried_part + inner_part,
    )


def stick_mixer(queries, key_rows, value_rows, offsets):
    seq_count, tok_rows, head_count, head_width = queries.shape
    own_index = lax.axis_index("sp")
    sp_count = lax.axis_size("sp")
    factor = 1.0 / math.sqrt(head_width)
    q_pos = own_index * tok_rows + lax.iota(jnp.int32, tok_rows)
    start_acc = jnp.zeros((sp_count, seq_count, tok_rows, head_count, head_width), jnp.float32)
    start_log = jnp.zeros((sp_count, seq_count, tok_rows, head_count), jnp.float32)

    def one_block(carried, key_blk, value_blk, slot):

        def compute(states):
            sums_acc, log_sums = states
            scores = jnp.einsum(
                "bqhe,bkhe->bhqk", queries, key_blk, preferred_element_type=jnp.float32
            )
            scores = scores * factor + offsets[None, :, None, None]
            k_pos = slot * tok_rows + lax.iota(jnp.int32, tok_rows)
            strict = k_pos[None, :] < q_pos[:, None]
            log_keep = jnp.where(strict, jax.nn.log_sigmoid(-scores), 0.0)
            inner_sum = lax.cumsum(log_keep, axis=3, reverse=True) - log_keep
            sticks = jnp.where(strict, jnp.exp(jax.nn.log_sigmoid(scores) + inner_sum), 0.0).astype(
                jnp.bfloat16
            )
            partial_value = jnp.einsum(
                "bhqk,bkhe->bqhe", sticks, value_blk, preferred_element_type=jnp.float32
            )
            totals = jnp.transpose(jnp.sum(log_keep, axis=3), (0, 2, 1))
            return (
                lax.dynamic_update_index_in_dim(sums_acc, partial_value, slot, 0),
                lax.dynamic_update_index_in_dim(log_sums, totals, slot, 0),
            )

        return lax.cond(slot <= own_index, compute, lambda states: states, carried)

    key_all = lax.all_gather(key_rows, "sp", axis=1, tiled=True)
    value_all = lax.all_gather(value_rows, "sp", axis=1, tiled=True)
    blocks = key_all.shape[1] // tok_rows

    def turn(block_idx, states):
        key_blk = lax.dynamic_slice_in_dim(key_all, block_idx * tok_rows, tok_rows, 1)
        value_blk = lax.dynamic_slice_in_dim(value_all, block_idx * tok_rows, tok_rows, 1)
        return one_block(states, key_blk, value_blk, block_idx)

    sums_acc, log_sums = lax.fori_loop(0, blocks, turn, (start_acc, start_log))
    later_sum = jnp.cumsum(log_sums[::-1], axis=0)[::-1] - log_sums
    return jnp.sum(sums_acc * jnp.exp(later_sum)[..., None], axis=0).astype(jnp.bfloat16)


def combine_states(earlier, later):
    return (earlier[0] + later[0], jnp.exp(later[0])[..., None] * earlier[1] + later[1])


def recur_mixer(queries, gate_pre, inputs, rooms, gain):
    seq_count, tok_rows, head_count, key_dim = queries.shape
    val_dim = inputs.shape[3]
    key_in = rooms * jax.nn.sigmoid(-gate_pre.astype(jnp.float32))
    log_forget = jnp.log1p(-key_in)
    query32 = queries.astype(jnp.float32)
    blocks = tok_rows // REC_BLOCK

    def split_blocks(tensor):
        return jnp.transpose(
            tensor.reshape(seq_count, blocks, REC_BLOCK, head_count, tensor.shape[3]),
            (1, 0, 3, 2, 4),
        )

    empty_state = jnp.zeros((seq_count, head_count, key_dim, val_dim), jnp.float32)
    final_state, pieces = lax.scan(
        block_step,
        empty_state,
        (
            split_blocks(query32),
            split_blocks(key_in),
            split_blocks(inputs.astype(jnp.float32)),
            split_blocks(log_forget),
        ),
    )
    local_out = jnp.transpose(pieces, (1, 0, 3, 2, 4)).reshape(
        seq_count, tok_rows, head_count, val_dim
    )
    running = jnp.cumsum(log_forget, axis=1)
    identity = (jnp.zeros((seq_count, head_count, key_dim), jnp.float32), empty_state)
    incoming = carried_in((running[:, -1], final_state), "sp", combine_states, identity)[1]
    raw_out = local_out + jnp.einsum(
        "bthk,bhkv->bthv", query32 * jnp.exp(running), incoming, precision=highest
    )
    factor = lax.rsqrt(jnp.mean(raw_out * raw_out, axis=3, keepdims=True) + norm_eps)
    return (raw_out * factor * gain).astype(jnp.bfloat16)


def body(
    tokens,
    mix_gain,
    attn_query,
    attn_key,
    attn_value,
    rec_query,
    rec_forget,
    rec_input,
    break_offset,
    forget_room,
    out_gain,
    out_attn,
    out_rec,
):
    whole = lax.all_gather(tokens, "tp", axis=2, tiled=True)
    seq_rows = whole.shape[1]
    model_width = whole.shape[2]
    rows32 = whole.astype(jnp.float32)
    factor = lax.rsqrt(jnp.mean(rows32 * rows32, axis=2, keepdims=True) + norm_eps)
    normed = (rows32 * factor * mix_gain).astype(jnp.bfloat16).reshape(seq_rows, model_width)
    weights = (attn_query, attn_key, attn_value, rec_query, rec_forget, rec_input)
    turned = (
        lax.all_to_all(weights[0], "fs", split_axis=1, concat_axis=0, tiled=True),
        lax.all_to_all(weights[1], "fs", split_axis=1, concat_axis=0, tiled=True),
        lax.all_to_all(weights[2], "fs", split_axis=1, concat_axis=0, tiled=True),
        lax.all_to_all(weights[3], "fs", split_axis=1, concat_axis=0, tiled=True),
        lax.all_to_all(weights[4], "fs", split_axis=1, concat_axis=0, tiled=True),
        lax.all_to_all(weights[5], "fs", split_axis=1, concat_axis=0, tiled=True),
    )
    pieces = lax.all_gather(normed, "fs", axis=0, tiled=True)
    projected = tuple(
        (
            jnp.dot(pieces, matrix, preferred_element_type=jnp.float32).astype(jnp.bfloat16)
            for matrix in turned
        )
    )
    seq_count = lax.axis_size("fs")
    own_fs = lax.axis_index("fs")
    attn_heads = break_offset.shape[0] // seq_count
    rec_heads = forget_room.shape[0] // seq_count
    offsets = lax.dynamic_slice_in_dim(break_offset, own_fs * attn_heads, attn_heads, 0)
    rooms = lax.dynamic_slice_in_dim(forget_room, own_fs * rec_heads, rec_heads, 0)

    def heads_of(matrix, width_each):
        return matrix.reshape(seq_count, seq_rows, matrix.shape[1] // width_each, width_each)

    attn_out = stick_mixer(
        heads_of(projected[0], HEAD),
        heads_of(projected[1], HEAD),
        heads_of(projected[2], HEAD),
        offsets,
    )
    rec_out = recur_mixer(
        heads_of(projected[3], DK),
        heads_of(projected[4], DK),
        heads_of(projected[5], DV),
        rooms,
        out_gain,
    )
    attn_flat = attn_out.reshape(seq_count * seq_rows, -1)
    rec_flat = rec_out.reshape(seq_count * seq_rows, -1)
    attn_flat, rec_flat = (
        lax.all_to_all(attn_flat, "fs", split_axis=0, concat_axis=1, tiled=True),
        lax.all_to_all(rec_flat, "fs", split_axis=0, concat_axis=1, tiled=True),
    )
    full_attn, full_rec = (
        lax.all_gather(out_attn, "fs", axis=1, tiled=True),
        lax.all_gather(out_rec, "fs", axis=1, tiled=True),
    )
    share = seq_rows // lax.axis_size("tp")
    mixed = lax.psum_scatter(
        (
            jnp.dot(attn_flat, full_attn, preferred_element_type=jnp.float32)
            + jnp.dot(rec_flat, full_rec, preferred_element_type=jnp.float32)
        ).astype(jnp.bfloat16),
        "tp",
        scatter_dimension=0,
        tiled=True,
    )
    return mixed.reshape(1, share, model_width)


def solution(mesh):
    placed = (
        P(("grp", "fs"), "sp", "tp"),
        P(),
        P("fs", "tp"),
        P("fs", "tp"),
        P("fs", "tp"),
        P("fs", "tp"),
        P("fs", "tp"),
        P("fs", "tp"),
        P("tp"),
        P("tp", None),
        P(),
        P("tp", "fs"),
        P("tp", "fs"),
    )
    return jax.shard_map(
        body,
        mesh=mesh,
        in_specs=placed,
        out_specs=P(("grp", "fs"), ("sp", "tp"), None),
        check_vma=False,
    )
```

profile of v0, /device:TPU:0, one launch (start us, length us, event | category | flops | bytes accessed | tf_op | source)
XLA Modules:
  0.0 285.6 jit_solution(8007163119693888808)
XLA Ops:
  6.5 2.6 all_gather.28
  9.4 1.7 fusion.54
  11.1 1.3 copy.92
  12.4 4.1 %all-to-all-start.4 = ((bf16[1024,2,256]{0,2,1:T(8,128)(2,1)}), bf16[1024,2,256]{0,2,1:T(8,128)(2,1)S(1)}, u32[]{:S(2)}, u32[]{:S(2)}) async-start(bf16[1024,2,256]{0,2,1:T(8,128)(2,1)} %bitcast.20), calls=%async_computation.4 | async-start | bytes 2097152 | tf_op jit(solution)/shard_map/all_to_all | solution.py:175
  17.9 21.6 %all-to-all-done.4 = bf16[1024,2,256]{0,2,1:T(8,128)(2,1)S(1)} async-done(((bf16[1024,2,256]{0,2,1:T(8,128)(2,1)}), bf16[1024,2,256]{0,2,1:T(8,128)(2,1)S(1)}, u32[]{:S(2)}, u32[]{:S(2)}) %all-to-all-start.4) | async-done | bytes 1048608 | tf_op jit(solution)/shard_map/all_to_all | solution.py:175
  39.4 3.6 %all-to-all-start.6 = ((bf16[1024,2,256]{0,2,1:T(8,128)(2,1)}), bf16[1024,2,256]{0,2,1:T(8,128)(2,1)S(1)}, u32[]{:S(2)}, u32[]{:S(2)}) async-start(bf16[1024,2,256]{0,2,1:T(8,128)(2,1)} %bitcast.29), calls=%async_computation.6 | async-start | bytes 2097152 | tf_op jit(solution)/shard_map/all_to_all | solution.py:174
  45.1 10.5 %all-to-all-done.6 = bf16[1024,2,256]{0,2,1:T(8,128)(2,1)S(1)} async-done(((bf16[1024,2,256]{0,2,1:T(8,128)(2,1)}), bf16[1024,2,256]{0,2,1:T(8,128)(2,1)S(1)}, u32[]{:S(2)}, u32[]{:S(2)}) %all-to-all-start.6) | async-done | bytes 1048608 | tf_op jit(solution)/shard_map/all_to_all | solution.py:174
  55.6 3.6 %all-to-all-start.5 = ((bf16[1024,2,256]{0,2,1:T(8,128)(2,1)}), bf16[1024,2,256]{0,2,1:T(8,128)(2,1)S(1)}, u32[]{:S(2)}, u32[]{:S(2)}) async-start(bf16[1024,2,256]{0,2,1:T(8,128)(2,1)} %bitcast.144), calls=%async_computation.5 | async-start | bytes 2097152 | tf_op jit(solution)/shard_map/all_to_all | solution.py:176
  59.2 2.3 copy.82
  61.5 22.8 %all-to-all-done.5 = bf16[1024,2,256]{0,2,1:T(8,128)(2,1)S(1)} async-done(((bf16[1024,2,256]{0,2,1:T(8,128)(2,1)}), bf16[1024,2,256]{0,2,1:T(8,128)(2,1)S(1)}, u32[]{:S(2)}, u32[]{:S(2)}) %all-to-all-start.5) | async-done | bytes 1048608 | tf_op jit(solution)/shard_map/all_to_all | solution.py:176
  84.3 4.4 %all-to-all-start = ((bf16[1024,2,256]{0,2,1:T(8,128)(2,1)}), bf16[1024,2,256]{0,2,1:T(8,128)(2,1)}, u32[]{:S(2)}, u32[]{:S(2)}) async-start(bf16[1024,2,256]{0,2,1:T(8,128)(2,1)} %bitcast.145), calls=%async_computation | async-start | bytes 2097152 | tf_op jit(solution)/shard_map/all_to_all | solution.py:172
  88.7 2.3 copy.87
  91.1 12.6 %all-to-all-done = bf16[1024,2,256]{0,2,1:T(8,128)(2,1)} async-done(((bf16[1024,2,256]{0,2,1:T(8,128)(2,1)}), bf16[1024,2,256]{0,2,1:T(8,128)(2,1)}, u32[]{:S(2)}, u32[]{:S(2)}) %all-to-all-start) | async-done | bytes 1048608 | tf_op jit(solution)/shard_map/all_to_all | solution.py:172
  103.7 4.5 %all-to-all-start.2 = ((bf16[1024,2,256]{0,2,1:T(8,128)(2,1)}), bf16[1024,2,256]{0,2,1:T(8,128)(2,1)}, u32[]{:S(2)}, u32[]{:S(2)}) async-start(bf16[1024,2,256]{0,2,1:T(8,128)(2,1)} %bitcast.146), calls=%async_computation.2 | async-start | bytes 2097152 | tf_op jit(solution)/shard_map/all_to_all | solution.py:173
  108.1 2.3 copy.85
  110.4 10.6 %all-to-all-done.2 = bf16[1024,2,256]{0,2,1:T(8,128)(2,1)} async-done(((bf16[1024,2,256]{0,2,1:T(8,128)(2,1)}), bf16[1024,2,256]{0,2,1:T(8,128)(2,1)}, u32[]{:S(2)}, u32[]{:S(2)}) %all-to-all-start.2) | async-done | bytes 1048608 | tf_op jit(solution)/shard_map/all_to_all | solution.py:173
  121.1 4.4 %all-to-all-start.1 = ((bf16[1024,2,256]{0,2,1:T(8,128)(2,1)}), bf16[1024,2,256]{0,2,1:T(8,128)(2,1)}, u32[]{:S(2)}, u32[]{:S(2)}) async-start(bf16[1024,2,256]{0,2,1:T(8,128)(2,1)} %bitcast.141), calls=%async_computation.1 | async-start | bytes 2097152 | tf_op jit(solution)/shard_map/all_to_all | solution.py:171
  126.3 1.3 copy.93
  129.0 1.4 copy.96
  130.3 2.3 copy.83
  132.6 2.4 copy.88
  134.9 2.6 all-to-all-done.1
  137.5 1.5 copy.86
  139.1 2.5 fusion.51
  141.6 1.8 div.26
  143.4 1.9 div.27
  145.3 2.4 fusion.46
  147.7 1.8 reshape.147
  149.4 1.8 reshape.145
  153.4 1.8 fusion.66
  156.2 6.9 %while.43 = (s32[]{:T(128)}, f32[2,2,128,128]{3,2,1,0:T(8,128)S(1)}, f32[2,2,2,64,128]{4,3,0,2,1:T(8,128)}, f32[2,2,2,64,128]{4,3,2,1,0:T(8,128)}, f32[2,2,2,64,...) while((s32[]{:T(128)}, ...), condition=%wide.region_11.12_spmd.clone, body=%wide.region_9.11_spmd.clone.sunk | while | flops 153571328 | bytes 3239036 | solution.py:125
  163.1 16.6 %all-gather.2 = bf16[8,2,128,128]{3,2,1,0:T(8,128)(2,1)} all-gather(bf16[2,2,128,128]{3,2,1,0:T(8,128)(2,1)S(1)} %convert_element_type.118), channel_id=4, replica_groups=mesh['grp'=2,'sp'=4,'fs'=2,'tp'=2] {'sp'}, dimensions={0}, use_global_device_ids=true | all-gather | bytes 655360 | tf_op jit(solution)/shard_map/all_gather | solution.py:18
  179.8 2.3 exponential_multiply_fusion
  182.0 9.4 %all-gather.1 = bf16[8,1,2,128]{3,2,1,0:T(2,128)(2,1)S(1)} all-gather(bf16[2,1,2,128]{3,2,1,0:T(2,128)(2,1)S(1)} %slice.12), channel_id=3, replica_groups=mesh['grp'=2,'sp'=4,'fs'=2,'tp'=2] {'sp'}, dimensions={0}, use_global_device_ids=true | all-gather | bytes 5120 | tf_op jit(solution)/shard_map/all_gather | solution.py:18
  191.5 1.8 copy.104
  193.3 1.7 convolution_convert_fusion.5
  195.0 16.5 %all_gather.30 = bf16[2,512,2,128]{3,1,2,0:T(8,128)(2,1)} all-gather(bf16[2,128,2,128]{3,1,2,0:T(8,128)(2,1)S(1)} %copy.84), channel_id=1, replica_groups=mesh['grp'=2,'sp'=4,'fs'=2,'tp'=2] {'sp'}, dimensions={1}, use_global_device_ids=true | all-gather | bytes 655360 | tf_op jit(solution)/shard_map/all_gather | solution.py:92
  212.1 14.9 %all_gather.31 = bf16[2,512,2,128]{3,1,2,0:T(8,128)(2,1)S(1)} all-gather(bf16[2,128,2,128]{3,1,2,0:T(8,128)(2,1)S(1)} %copy.89), channel_id=1, replica_groups=mesh['grp'=2,'sp'=4,'fs'=2,'tp'=2] {'sp'}, dimensions={1}, use_global_device_ids=true | all-gather | bytes 655360 | tf_op jit(solution)/shard_map/all_gather | solution.py:93
  227.6 6.6 %while.42 = (s32[]{:T(128)}, f32[4,2,128,2,128]{4,2,3,1,0:T(8,128)S(1)}, f32[4,2,128,2]{2,3,1,0:T(2,128)S(1)}, s32[]{:T(128)}, bf16[2,512,2,128]{3,1,2,0:T(8,128...) while((s32[]{:T(128)}, ...), condition=%wide.region_6.7_spmd.clone, body=%wide.region_1.6_spmd.clone.sunk | while | flops 43925260 | bytes 2286935 | solution.py:101
  227.7 6.4 %conditional.3 = ((f32[4,2,128,2,128]{4,2,3,1,0:T(8,128)S(1)}, f32[4,2,128,2]{2,3,1,0:T(2,128)S(1)})) conditional(s32[]{:T(128)} %convert_element_type.168, (f32[4,2,128,2,128]{4,2,3,1,0:T(8,128)S(1)}, f32[4,2,128,2]{2,3,1,0:T(2,128)S(1)}) %tuple.100, (s32[]{:T(128)}, s32[]{:T(128)}, bf16[2,512,2,128]{3,1,2,0:T(8,128)(2,1)}, ...), branch_computations={%region_2.0_spmd, %region_3.5_spmd} | conditional | flops 43925256 | bytes 2286220 | solution.py:90
  229.1 4.4 %reduce_window_sum.43 = f32[2,2,128,128]{2,3,1,0:T(8,128)S(1)} reduce-window(f32[2,2,128,128]{2,3,1,0:T(8,128)S(1)} %get-tuple-element.514, f32[]{:T(128)} %constant.131.clone), window={size=1x1x1x128 pad=0_0x0_0x0_0x0_127}, to_apply=%region_4.3 | reduce-window | flops 8323072 | bytes 524292 | tf_op jit(solution)/shard_map/while/body/eval_jaxpr/cond/branch_1_fun/reduce_window_sum | solution.py:77
  235.5 3.4 %all-to-all-start.3 = ((bf16[2,128,256]{1,2,0:T(8,128)(2,1)}), bf16[2,128,256]{1,2,0:T(8,128)(2,1)S(1)}, u32[]{:S(2)}, u32[]{:S(2)}) async-start(bf16[2,128,256]{1,2,0:T(8,128)(2,1)} %bitcast.17), calls=%async_computation.3 | async-start | bytes 262144 | tf_op jit(solution)/shard_map/all_to_all | solution.py:211
  240.3 3.0 %all-to-all-done.3 = bf16[2,128,256]{1,2,0:T(8,128)(2,1)S(1)} async-done(((bf16[2,128,256]{1,2,0:T(8,128)(2,1)}), bf16[2,128,256]{1,2,0:T(8,128)(2,1)S(1)}, u32[]{:S(2)}, u32[]{:S(2)}) %all-to-all-start.3) | async-done | bytes 131104 | tf_op jit(solution)/shard_map/all_to_all | solution.py:211
  243.3 3.4 %all-to-all-start.7 = ((bf16[2,128,256]{1,2,0:T(8,128)(2,1)}), bf16[2,128,256]{1,2,0:T(8,128)(2,1)S(1)}, u32[]{:S(2)}, u32[]{:S(2)}) async-start(bf16[2,128,256]{1,2,0:T(8,128)(2,1)} %bitcast.38), calls=%async_computation.7 | async-start | bytes 262144 | tf_op jit(solution)/shard_map/all_to_all | solution.py:212
  246.8 2.1 fusion.69
  248.8 2.3 all-to-all-done.7
  251.1 2.9 %fusion.44 = bf16[128,2048]{1,0:T(8,128)(2,1)} fusion(f32[128,2048]{1,0:T(8,128)S(1)} %fusion.69, bf16[128,512]{0,1:T(8,128)(2,1)S(1)} %bitcast.150, bf16[512,2048]{1,0:T(8,128)(2,1)} %all-gather.9.cloned.1.call-done), kind=kOutput, calls=%fused_computation.60 | convolution fusion | flops 268959744 | bytes 3801088 | tf_op jit(solution)/shard_map/dot_general | solution.py:222
  254.0 25.0 %reduce-scatter.2.cloned.1.call-done = bf16[64,2048]{1,0:T(8,128)(2,1)} async-done(((bf16[128,2048]{1,0:T(8,128)(2,1)}), bf16[64,2048]{1,0:T(8,128)(2,1)}) %reduce-scatter.2.cloned.1.call-update) | async-done | bytes 262160 | tf_op jit(solution)/shard_map/reduce_scatter | solution.py:219
  (99 shorter events, 21.5 us)
Async XLA Ops:
  6.5 119.8 %copy-start = (f32[4,128]{1,0:T(4,128)S(1)}, f32[4,128]{1,0:T(4,128)}, u32[]{:S(2)}) copy-start(f32[4,128]{1,0:T(4,128)} %param.30) | copy-start | bytes 6148
  6.5 4.5 %copy-start.4 = (bf16[1024,512]{1,0:T(8,128)(2,1)S(1)}, bf16[1024,512]{1,0:T(8,128)(2,1)}, u32[]{:S(2)}) copy-start(bf16[1024,512]{1,0:T(8,128)(2,1)} %param.27) | copy-start | bytes 3145732
  6.5 132.5 %all-gather.11.cloned.1.call-start = ((), (), s32[]{:S(2)}) async-start(), calls=%async_computation.12 | async-start | bytes 1572864 | tf_op jit(solution)/shard_map/all_gather | solution.py:178
  11.1 5.5 %copy-start.5 = (bf16[1024,512]{1,0:T(8,128)(2,1)S(1)}, bf16[1024,512]{1,0:T(8,128)(2,1)}, u32[]{:S(2)}) copy-start(bf16[1024,512]{1,0:T(8,128)(2,1)} %param.26) | copy-start | bytes 3145732
  12.4 27.0 %all-to-all-start.4 = ((bf16[1024,2,256]{0,2,1:T(8,128)(2,1)}), bf16[1024,2,256]{0,2,1:T(8,128)(2,1)S(1)}, u32[]{:S(2)}, u32[]{:S(2)}) async-start(bf16[1024,2,256]{0,2,1:T(8,128)(2,1)} %bitcast.20), calls=%async_computation.4 | async-start | bytes 2097152 | tf_op jit(solution)/shard_map/all_to_all | solution.py:175
  17.9 25.9 %copy-start.6 = (bf16[1024,512]{1,0:T(8,128)(2,1)S(1)}, bf16[1024,512]{1,0:T(8,128)(2,1)}, u32[]{:S(2)}) copy-start(bf16[1024,512]{1,0:T(8,128)(2,1)} %param.28) | copy-start | bytes 3145732
  39.4 16.2 %all-to-all-start.6 = ((bf16[1024,2,256]{0,2,1:T(8,128)(2,1)}), bf16[1024,2,256]{0,2,1:T(8,128)(2,1)S(1)}, u32[]{:S(2)}, u32[]{:S(2)}) async-start(bf16[1024,2,256]{0,2,1:T(8,128)(2,1)} %bitcast.29), calls=%async_computation.6 | async-start | bytes 2097152 | tf_op jit(solution)/shard_map/all_to_all | solution.py:174
  43.0 203.7 %all-gather.7.cloned.1.call-start = ((), (), s32[]{:S(2)}) async-start(), calls=%async_computation.9 | async-start | bytes 3145728 | tf_op jit(solution)/shard_map/all_gather | solution.py:215
  55.6 28.7 %all-to-all-start.5 = ((bf16[1024,2,256]{0,2,1:T(8,128)(2,1)}), bf16[1024,2,256]{0,2,1:T(8,128)(2,1)S(1)}, u32[]{:S(2)}, u32[]{:S(2)}) async-start(bf16[1024,2,256]{0,2,1:T(8,128)(2,1)} %bitcast.144), calls=%async_computation.5 | async-start | bytes 2097152 | tf_op jit(solution)/shard_map/all_to_all | solution.py:176
  84.3 19.3 %all-to-all-start = ((bf16[1024,2,256]{0,2,1:T(8,128)(2,1)}), bf16[1024,2,256]{0,2,1:T(8,128)(2,1)}, u32[]{:S(2)}, u32[]{:S(2)}) async-start(bf16[1024,2,256]{0,2,1:T(8,128)(2,1)} %bitcast.145), calls=%async_computation | async-start | bytes 2097152 | tf_op jit(solution)/shard_map/all_to_all | solution.py:172
  103.7 17.4 %all-to-all-start.2 = ((bf16[1024,2,256]{0,2,1:T(8,128)(2,1)}), bf16[1024,2,256]{0,2,1:T(8,128)(2,1)}, u32[]{:S(2)}, u32[]{:S(2)}) async-start(bf16[1024,2,256]{0,2,1:T(8,128)(2,1)} %bitcast.146), calls=%async_computation.2 | async-start | bytes 2097152 | tf_op jit(solution)/shard_map/all_to_all | solution.py:173
  110.4 15.8 %copy-start.11 = (f32[4]{0:T(128)S(1)}, f32[4]{0:T(128)}, u32[]{:S(2)}) copy-start(f32[4]{0:T(128)} %param.29) | copy-start | bytes 52
  121.1 16.5 %all-to-all-start.1 = ((bf16[1024,2,256]{0,2,1:T(8,128)(2,1)}), bf16[1024,2,256]{0,2,1:T(8,128)(2,1)}, u32[]{:S(2)}, u32[]{:S(2)}) async-start(bf16[1024,2,256]{0,2,1:T(8,128)(2,1)} %bitcast.141), calls=%async_computation.1 | async-start | bytes 2097152 | tf_op jit(solution)/shard_map/all_to_all | solution.py:171
  125.5 125.7 %all-gather.9.cloned.1.call-start = ((), (), s32[]{:S(2)}) async-start(), calls=%async_computation.10 | async-start | bytes 3145728 | tf_op jit(solution)/shard_map/all_gather | solution.py:216
  132.6 6.5 %copy-start.7 = (bf16[2,1024,256]{2,1,0:T(8,128)(2,1)S(1)}, bf16[2,1024,256]{2,1,0:T(8,128)(2,1)}, u32[]{:S(2)}) copy-start(bf16[2,1024,256]{2,1,0:T(8,128)(2,1)} %copy.93) | copy-start | bytes 3145732
  139.1 6.2 %copy-start.1 = (bf16[1,256,2048]{2,1,0:T(8,128)(2,1)S(1)}, bf16[1,256,2048]{2,1,0:T(8,128)(2,1)}, u32[]{:S(2)}) copy-start(bf16[1,256,2048]{2,1,0:T(8,128)(2,1)} %all-gather.11.cloned.1.call-done) | copy-start | bytes 3145732
  143.4 7.8 %copy-start.3 = (bf16[2,1024,256]{2,1,0:T(8,128)(2,1)S(1)}, bf16[2,1024,256]{2,1,0:T(8,128)(2,1)}, u32[]{:S(2)}) copy-start(bf16[2,1024,256]{2,1,0:T(8,128)(2,1)} %copy.96) | copy-start | bytes 3145732
  182.0 29.5 %copy-start.2 = (bf16[2,1024,256]{2,1,0:T(8,128)(2,1)S(1)}, bf16[2,1024,256]{2,1,0:T(8,128)(2,1)}, u32[]{:S(2)}) copy-start(bf16[2,1024,256]{2,1,0:T(8,128)(2,1)} %copy.88) | copy-start | bytes 3145732
  234.7 4.2 %copy-start.8 = (f32[2,128,2,128]{1,3,2,0:T(8,128)S(1)}, f32[2,128,2,128]{1,3,2,0:T(8,128)}, u32[]{:S(2)}) copy-start(f32[2,128,2,128]{1,3,2,0:T(8,128)} %copy.104) | copy-start | bytes 786436
  234.7 4.2 %copy-start.9 = (f32[2,128,2,128]{3,2,1,0:T(2,128)S(1)}, f32[2,128,2,128]{3,2,1,0:T(2,128)}, u32[]{:S(2)}) copy-start(f32[2,128,2,128]{3,2,1,0:T(2,128)} %get-tuple-element.520) | copy-start | bytes 786436
  235.5 7.8 %all-to-all-start.3 = ((bf16[2,128,256]{1,2,0:T(8,128)(2,1)}), bf16[2,128,256]{1,2,0:T(8,128)(2,1)S(1)}, u32[]{:S(2)}, u32[]{:S(2)}) async-start(bf16[2,128,256]{1,2,0:T(8,128)(2,1)} %bitcast.17), calls=%async_computation.3 | async-start | bytes 262144 | tf_op jit(solution)/shard_map/all_to_all | solution.py:211
  238.9 0.7 copy-start.10
  243.3 7.8 %all-to-all-start.7 = ((bf16[2,128,256]{1,2,0:T(8,128)(2,1)}), bf16[2,128,256]{1,2,0:T(8,128)(2,1)S(1)}, u32[]{:S(2)}, u32[]{:S(2)}) async-start(bf16[2,128,256]{1,2,0:T(8,128)(2,1)} %bitcast.38), calls=%async_computation.7 | async-start | bytes 262144 | tf_op jit(solution)/shard_map/all_to_all | solution.py:212
  246.7 32.4 %reduce-scatter.2.cloned.1.call-start = ((), (), s32[]{:S(2)}) async-start(), calls=%async_computation.11 | async-start | bytes 786432 | tf_op jit(solution)/shard_map/reduce_scatter | solution.py:219
Sparse Core Ops, SparseCore 0:
  11.2 31.5 all-gather.10
  45.4 49.9 all-gather.6
  127.8 34.1 all-gather.8
  254.2 24.8 reduce-scatter.1
where the time goes:
time: 287 us; the launch traced here: 286 us
  waiting for transfers between devices  112 us (39%)
  blocking collectives  60.2 us (21%)
  local copies, waits for them, and re-layouts  35.2 us (12%)
  starting transfers between devices  31.5 us (11%)
  matrix products  20.6 us (7%)
  between operations  13.5 us (5%)
  other arithmetic  11.9 us (4%)
    all_gather x2, blocking collectives, carried_in(): lax.all_gather(a.astype(kind), axis)  26.1 us
    reduce_scatter x1, waiting for transfers between devices, body(): lax.psum_scatter((jnp.dot(attn_flat, full_attn, preferred_element_type=jn...  25 us
    all_to_all x1, waiting for transfers between devices, body(): lax.all_to_all(weights[5], 'fs', split_axis=1, concat_axis=0, tiled=True)  22.8 us
    all_to_all x1, waiting for transfers between devices, body(): lax.all_to_all(weights[4], 'fs', split_axis=1, concat_axis=0, tiled=True)  21.6 us
    all_gather x1, blocking collectives, stick_mixer(): key_all = lax.all_gather(key_rows, 'sp', axis=1, tiled=True)  16.5 us
    all_gather x1, blocking collectives, stick_mixer(): value_all = lax.all_gather(value_rows, 'sp', axis=1, tiled=True)  14.9 us
    all_to_all x1, waiting for transfers between devices, body(): lax.all_to_all(weights[1], 'fs', split_axis=1, concat_axis=0, tiled=True)  12.6 us
    unnamed x31, local copies, waits for them, and re-layouts  10.9 us
  transfers between devices with their start and end apart: 12, of which 9 were waited for; matrix products, arithmetic and copies ran while one was open for 22% of the time, Pallas kernels for 0%

commit v1 on v0

--- a/solution.py
+++ b/solution.py
@@ -169,7 +169,15 @@
     weights = (attn_query, attn_key, attn_value, rec_query, rec_forget, rec_input)
     turned = (
         lax.all_to_all(weights[0], "fs", split_axis=1, concat_axis=0, tiled=True),
-        lax.all_to_all(weights[1], "fs", split_axis=1, concat_axis=0, tiled=True),
+        jnp.concatenate(
+            lax.all_to_all(
+                jnp.stack(jnp.split(weights[1], lax.psum(1, axis_name="fs"), 1), 0),
+                axis_name="fs",
+                split_axis=0,
+                concat_axis=0,
+            ),
+            0,
+        ),
         lax.all_to_all(weights[2], "fs", split_axis=1, concat_axis=0, tiled=True),
         lax.all_to_all(weights[3], "fs", split_axis=1, concat_axis=0, tiled=True),
         lax.all_to_all(weights[4], "fs", split_axis=1, concat_axis=0, tiled=True),

time: 287 us -> 273 us (0.951)
  waiting for transfers between devices: 112 us -> 101 us
  local copies, waits for them, and re-layouts: 35.2 us -> 29.3 us
    all_to_all x1, waiting for transfers between devices: 12.6 us -> 0.01 us  [body(): lax.all_to_all(jnp.stack(jnp.split(weights[1], lax.psum(1, axis_name='fs'...]
    unnamed x31 -> x32, local copies, waits for them, and re-layouts: 10.9 us -> 8.56 us
  transfers between devices with their start and end apart: 12 -> 12, of which waited for: 9 -> 8; matrix products, arithmetic and copies ran while one was open for 22% -> 21% of each run, Pallas kernels for 0% -> 0%
where the time goes in v1:
time: 273 us; the launch traced here: 271 us
  waiting for transfers between devices  101 us (37%)
  blocking collectives  61.3 us (22%)
  starting transfers between devices  32.6 us (12%)
  local copies, waits for them, and re-layouts  29.3 us (11%)
  matrix products  21.5 us (8%)
  between operations  13.5 us (5%)
  other arithmetic  12 us (4%)
    reduce_scatter x1, waiting for transfers between devices, body(): lax.psum_scatter((jnp.dot(attn_flat, full_attn, preferred_element_type=jn...  27.2 us
    all_gather x2, blocking collectives, carried_in(): lax.all_gather(a.astype(kind), axis)  26.7 us
    all_to_all x1, waiting for transfers between devices, body(): lax.all_to_all(weights[5], 'fs', split_axis=1, concat_axis=0, tiled=True)  22.7 us
    all_to_all x1, waiting for transfers between devices, body(): lax.all_to_all(weights[4], 'fs', split_axis=1, concat_axis=0, tiled=True)  20.9 us
    all_gather x1, blocking collectives, stick_mixer(): key_all = lax.all_gather(key_rows, 'sp', axis=1, tiled=True)  16.4 us
    all_gather x1, blocking collectives, stick_mixer(): value_all = lax.all_gather(value_rows, 'sp', axis=1, tiled=True)  15.6 us
    all_to_all x1, waiting for transfers between devices, body(): lax.all_to_all(weights[3], 'fs', split_axis=1, concat_axis=0, tiled=True)  12 us
    all_to_all x1, waiting for transfers between devices, body(): lax.all_to_all(weights[2], 'fs', split_axis=1, concat_axis=0, tiled=True)  9.1 us
  transfers between devices with their start and end apart: 12, of which 8 were waited for; matrix products, arithmetic and copies ran while one was open for 21% of the time, Pallas kernels for 0%

profile of v1, /device:TPU:0, one launch (start us, length us, event | category | flops | bytes accessed | tf_op | source)
XLA Modules:
  0.0 271.2 jit_solution(16683148303905917829)
XLA Ops:
  6.5 2.6 all_gather.28
  9.4 1.7 fusion.54
  11.1 1.3 copy.86
  12.5 4.2 %all-to-all-start.4 = ((bf16[1024,2,256]{0,2,1:T(8,128)(2,1)}), bf16[1024,2,256]{0,2,1:T(8,128)(2,1)S(1)}, u32[]{:S(2)}, u32[]{:S(2)}) async-start(bf16[1024,2,256]{0,2,1:T(8,128)(2,1)} %bitcast.20), calls=%async_computation.4 | async-start | bytes 2097152 | tf_op jit(solution)/shard_map/all_to_all | solution.py:183
  17.5 1.3 copy.92
  18.8 20.9 %all-to-all-done.4 = bf16[1024,2,256]{0,2,1:T(8,128)(2,1)S(1)} async-done(((bf16[1024,2,256]{0,2,1:T(8,128)(2,1)}), bf16[1024,2,256]{0,2,1:T(8,128)(2,1)S(1)}, u32[]{:S(2)}, u32[]{:S(2)}) %all-to-all-start.4) | async-done | bytes 1048608 | tf_op jit(solution)/shard_map/all_to_all | solution.py:183
  39.7 3.6 %all-to-all-start.6 = ((bf16[1024,2,256]{0,2,1:T(8,128)(2,1)}), bf16[1024,2,256]{0,2,1:T(8,128)(2,1)S(1)}, u32[]{:S(2)}, u32[]{:S(2)}) async-start(bf16[1024,2,256]{0,2,1:T(8,128)(2,1)} %bitcast.29), calls=%async_computation.6 | async-start | bytes 2097152 | tf_op jit(solution)/shard_map/all_to_all | solution.py:182
  43.3 1.3 copy.89
  44.6 12.0 %all-to-all-done.6 = bf16[1024,2,256]{0,2,1:T(8,128)(2,1)S(1)} async-done(((bf16[1024,2,256]{0,2,1:T(8,128)(2,1)}), bf16[1024,2,256]{0,2,1:T(8,128)(2,1)S(1)}, u32[]{:S(2)}, u32[]{:S(2)}) %all-to-all-start.6) | async-done | bytes 1048608 | tf_op jit(solution)/shard_map/all_to_all | solution.py:182
  56.6 3.6 %all-to-all-start.5 = ((bf16[1024,2,256]{0,2,1:T(8,128)(2,1)}), bf16[1024,2,256]{0,2,1:T(8,128)(2,1)S(1)}, u32[]{:S(2)}, u32[]{:S(2)}) async-start(bf16[1024,2,256]{0,2,1:T(8,128)(2,1)} %bitcast.145), calls=%async_computation.5 | async-start | bytes 2097152 | tf_op jit(solution)/shard_map/all_to_all | solution.py:184
  60.2 2.3 copy.81
  62.5 22.7 %all-to-all-done.5 = bf16[1024,2,256]{0,2,1:T(8,128)(2,1)S(1)} async-done(((bf16[1024,2,256]{0,2,1:T(8,128)(2,1)}), bf16[1024,2,256]{0,2,1:T(8,128)(2,1)S(1)}, u32[]{:S(2)}, u32[]{:S(2)}) %all-to-all-start.5) | async-done | bytes 1048608 | tf_op jit(solution)/shard_map/all_to_all | solution.py:184
  85.1 4.4 %all-to-all-start.2 = ((bf16[1024,2,256]{0,2,1:T(8,128)(2,1)}), bf16[1024,2,256]{0,2,1:T(8,128)(2,1)}, u32[]{:S(2)}, u32[]{:S(2)}) async-start(bf16[1024,2,256]{0,2,1:T(8,128)(2,1)} %bitcast.146), calls=%async_computation.2 | async-start | bytes 2097152 | tf_op jit(solution)/shard_map/all_to_all | solution.py:181
  89.5 2.3 copy.79
  91.8 9.1 %all-to-all-done.2 = bf16[1024,2,256]{0,2,1:T(8,128)(2,1)} async-done(((bf16[1024,2,256]{0,2,1:T(8,128)(2,1)}), bf16[1024,2,256]{0,2,1:T(8,128)(2,1)}, u32[]{:S(2)}, u32[]{:S(2)}) %all-to-all-start.2) | async-done | bytes 1048608 | tf_op jit(solution)/shard_map/all_to_all | solution.py:181
  100.9 4.5 %all-to-all-start.1 = ((bf16[1024,2,256]{0,2,1:T(8,128)(2,1)}), bf16[1024,2,256]{0,2,1:T(8,128)(2,1)}, u32[]{:S(2)}, u32[]{:S(2)}) async-start(bf16[1024,2,256]{0,2,1:T(8,128)(2,1)} %bitcast.142), calls=%async_computation.1 | async-start | bytes 2097152 | tf_op jit(solution)/shard_map/all_to_all | solution.py:171
  106.3 1.3 slice_bitcast_fusion.1
  108.6 1.3 copy.87
  110.0 1.3 copy.93
  111.3 1.3 copy.90
  112.6 1.5 copy.82
  114.1 1.8 all-to-all-done.1
  115.9 4.4 %all-to-all-start = ((bf16[2,1024,256]{2,1,0:T(8,128)(2,1)}), bf16[2,1024,256]{2,1,0:T(8,128)(2,1)}, u32[]{:S(2)}, u32[]{:S(2)}) async-start(bf16[2,1024,256]{2,1,0:T(8,128)(2,1)} %pad_maximum_fusion), calls=%async_computation | async-start | bytes 2097152 | tf_op jit(solution)/shard_map/all_to_all | solution.py:173
  120.4 2.3 copy.80
  122.6 2.5 fusion.51
  125.1 1.9 div.26
  127.0 2.4 fusion.46
  129.4 1.8 reshape.148
  133.4 1.8 fusion.66
  136.2 6.9 %while.43 = (s32[]{:T(128)}, f32[2,2,128,128]{3,2,1,0:T(8,128)S(1)}, f32[2,2,2,64,128]{4,3,0,2,1:T(8,128)}, f32[2,2,2,64,128]{4,3,2,1,0:T(8,128)}, f32[2,2,2,64,...) while((s32[]{:T(128)}, ...), condition=%wide.region_11.12_spmd.clone, body=%wide.region_9.11_spmd.clone.sunk | while | flops 153571328 | bytes 3239036 | solution.py:125
  145.3 1.3 exponential_multiply_fusion
  147.5 11.0 %all-gather.1 = bf16[8,1,2,128]{3,2,1,0:T(2,128)(2,1)S(1)} all-gather(bf16[2,1,2,128]{3,2,1,0:T(2,128)(2,1)S(1)} %slice.12), channel_id=3, replica_groups=mesh['grp'=2,'sp'=4,'fs'=2,'tp'=2] {'sp'}, dimensions={0}, use_global_device_ids=true | all-gather | bytes 5120 | tf_op jit(solution)/shard_map/all_gather | solution.py:18
  158.5 15.7 %all-gather.2 = bf16[8,2,128,128]{3,2,1,0:T(8,128)(2,1)} all-gather(bf16[2,2,128,128]{3,2,1,0:T(8,128)(2,1)S(1)} %convert_element_type.118), channel_id=4, replica_groups=mesh['grp'=2,'sp'=4,'fs'=2,'tp'=2] {'sp'}, dimensions={0}, use_global_device_ids=true | all-gather | bytes 655360 | tf_op jit(solution)/shard_map/all_gather | solution.py:18
  174.2 1.7 convolution_convert_fusion.5
  175.9 16.4 %all_gather.30 = bf16[2,512,2,128]{3,1,2,0:T(8,128)(2,1)} all-gather(bf16[2,128,2,128]{3,1,2,0:T(8,128)(2,1)S(1)} %copy.78), channel_id=1, replica_groups=mesh['grp'=2,'sp'=4,'fs'=2,'tp'=2] {'sp'}, dimensions={1}, use_global_device_ids=true | all-gather | bytes 655360 | tf_op jit(solution)/shard_map/all_gather | solution.py:92
  192.8 15.6 %all_gather.31 = bf16[2,512,2,128]{3,1,2,0:T(8,128)(2,1)} all-gather(bf16[2,128,2,128]{3,1,2,0:T(8,128)(2,1)S(1)} %copy.83), channel_id=1, replica_groups=mesh['grp'=2,'sp'=4,'fs'=2,'tp'=2] {'sp'}, dimensions={1}, use_global_device_ids=true | all-gather | bytes 655360 | tf_op jit(solution)/shard_map/all_gather | solution.py:93
  209.0 7.5 %while.42 = (s32[]{:T(128)}, f32[4,2,128,2,128]{4,2,3,1,0:T(8,128)S(1)}, f32[4,2,128,2]{2,3,1,0:T(2,128)S(1)}, s32[]{:T(128)}, bf16[2,512,2,128]{3,1,2,0:T(8,128...) while((s32[]{:T(128)}, ...), condition=%wide.region_6.7_spmd.clone, body=%wide.region_1.6_spmd.clone.sunk | while | flops 43925260 | bytes 2286935 | solution.py:101
  209.1 7.3 %conditional.3 = ((f32[4,2,128,2,128]{4,2,3,1,0:T(8,128)S(1)}, f32[4,2,128,2]{2,3,1,0:T(2,128)S(1)})) conditional(s32[]{:T(128)} %convert_element_type.168, (f32[4,2,128,2,128]{4,2,3,1,0:T(8,128)S(1)}, f32[4,2,128,2]{2,3,1,0:T(2,128)S(1)}) %tuple.101, (s32[]{:T(128)}, s32[]{:T(128)}, bf16[2,512,2,128]{3,1,2,0:T(8,128)(2,1)}, ...), branch_computations={%region_2.0_spmd, %region_3.5_spmd} | conditional | flops 43925256 | bytes 2286220 | solution.py:90
  209.2 1.3 fusion.20
  210.5 4.4 %reduce_window_sum.43 = f32[2,2,128,128]{2,3,1,0:T(8,128)S(1)} reduce-window(f32[2,2,128,128]{2,3,1,0:T(8,128)S(1)} %get-tuple-element.514, f32[]{:T(128)} %constant.131.clone), window={size=1x1x1x128 pad=0_0x0_0x0_0x0_127}, to_apply=%region_4.3 | reduce-window | flops 8323072 | bytes 524292 | tf_op jit(solution)/shard_map/while/body/eval_jaxpr/cond/branch_1_fun/reduce_window_sum | solution.py:77
  214.9 1.5 fusion.4
  217.8 4.4 %all-to-all-start.3 = ((bf16[2,128,256]{1,2,0:T(8,128)(2,1)}), bf16[2,128,256]{1,2,0:T(8,128)(2,1)S(1)}, u32[]{:S(2)}, u32[]{:S(2)}) async-start(bf16[2,128,256]{1,2,0:T(8,128)(2,1)} %bitcast.17), calls=%async_computation.3 | async-start | bytes 262144 | tf_op jit(solution)/shard_map/all_to_all | solution.py:219
  223.6 3.1 %all-to-all-done.3 = bf16[2,128,256]{1,2,0:T(8,128)(2,1)S(1)} async-done(((bf16[2,128,256]{1,2,0:T(8,128)(2,1)}), bf16[2,128,256]{1,2,0:T(8,128)(2,1)S(1)}, u32[]{:S(2)}, u32[]{:S(2)}) %all-to-all-start.3) | async-done | bytes 131104 | tf_op jit(solution)/shard_map/all_to_all | solution.py:219
  226.7 3.4 %all-to-all-start.7 = ((bf16[2,128,256]{1,2,0:T(8,128)(2,1)}), bf16[2,128,256]{1,2,0:T(8,128)(2,1)S(1)}, u32[]{:S(2)}, u32[]{:S(2)}) async-start(bf16[2,128,256]{1,2,0:T(8,128)(2,1)} %bitcast.38), calls=%async_computation.7 | async-start | bytes 262144 | tf_op jit(solution)/shard_map/all_to_all | solution.py:220
  230.2 2.1 fusion.69
  232.2 2.3 all-to-all-done.7
  234.6 2.9 %fusion.44 = bf16[128,2048]{1,0:T(8,128)(2,1)} fusion(f32[128,2048]{1,0:T(8,128)S(1)} %fusion.69, bf16[128,512]{0,1:T(8,128)(2,1)S(1)} %bitcast.150, bf16[512,2048]{1,0:T(8,128)(2,1)} %all-gather.9.cloned.1.call-done), kind=kOutput, calls=%fused_computation.60 | convolution fusion | flops 268959744 | bytes 3801088 | tf_op jit(solution)/shard_map/dot_general | solution.py:230
  237.5 27.2 %reduce-scatter.2.cloned.1.call-done = bf16[64,2048]{1,0:T(8,128)(2,1)} async-done(((bf16[128,2048]{1,0:T(8,128)(2,1)}), bf16[64,2048]{1,0:T(8,128)(2,1)}) %reduce-scatter.2.cloned.1.call-update) | async-done | bytes 262160 | tf_op jit(solution)/shard_map/reduce_scatter | solution.py:227
  (101 shorter events, 19.9 us)
Async XLA Ops:
  6.5 99.7 %copy-start = (f32[4,128]{1,0:T(4,128)S(1)}, f32[4,128]{1,0:T(4,128)}, u32[]{:S(2)}) copy-start(f32[4,128]{1,0:T(4,128)} %param.30) | copy-start | bytes 6148
  6.5 4.6 %copy-start.4 = (bf16[1024,512]{1,0:T(8,128)(2,1)S(1)}, bf16[1024,512]{1,0:T(8,128)(2,1)}, u32[]{:S(2)}) copy-start(bf16[1024,512]{1,0:T(8,128)(2,1)} %param.27) | copy-start | bytes 3145732
  6.5 116.1 %all-gather.11.cloned.1.call-start = ((), (), s32[]{:S(2)}) async-start(), calls=%async_computation.12 | async-start | bytes 1572864 | tf_op jit(solution)/shard_map/all_gather | solution.py:186
  12.5 5.0 %copy-start.5 = (bf16[1024,512]{1,0:T(8,128)(2,1)S(1)}, bf16[1024,512]{1,0:T(8,128)(2,1)}, u32[]{:S(2)}) copy-start(bf16[1024,512]{1,0:T(8,128)(2,1)} %param.26) | copy-start | bytes 3145732
  12.5 27.2 %all-to-all-start.4 = ((bf16[1024,2,256]{0,2,1:T(8,128)(2,1)}), bf16[1024,2,256]{0,2,1:T(8,128)(2,1)S(1)}, u32[]{:S(2)}, u32[]{:S(2)}) async-start(bf16[1024,2,256]{0,2,1:T(8,128)(2,1)} %bitcast.20), calls=%async_computation.4 | async-start | bytes 2097152 | tf_op jit(solution)/shard_map/all_to_all | solution.py:183
  16.7 213.5 %all-gather.7.cloned.1.call-start = ((), (), s32[]{:S(2)}) async-start(), calls=%async_computation.9 | async-start | bytes 3145728 | tf_op jit(solution)/shard_map/all_gather | solution.py:223
  17.4 25.8 %copy-start.6 = (bf16[1024,512]{1,0:T(8,128)(2,1)S(1)}, bf16[1024,512]{1,0:T(8,128)(2,1)}, u32[]{:S(2)}) copy-start(bf16[1024,512]{1,0:T(8,128)(2,1)} %param.28) | copy-start | bytes 3145732
  39.7 16.9 %all-to-all-start.6 = ((bf16[1024,2,256]{0,2,1:T(8,128)(2,1)}), bf16[1024,2,256]{0,2,1:T(8,128)(2,1)S(1)}, u32[]{:S(2)}, u32[]{:S(2)}) async-start(bf16[1024,2,256]{0,2,1:T(8,128)(2,1)} %bitcast.29), calls=%async_computation.6 | async-start | bytes 2097152 | tf_op jit(solution)/shard_map/all_to_all | solution.py:182
  56.6 28.5 %all-to-all-start.5 = ((bf16[1024,2,256]{0,2,1:T(8,128)(2,1)}), bf16[1024,2,256]{0,2,1:T(8,128)(2,1)S(1)}, u32[]{:S(2)}, u32[]{:S(2)}) async-start(bf16[1024,2,256]{0,2,1:T(8,128)(2,1)} %bitcast.145), calls=%async_computation.5 | async-start | bytes 2097152 | tf_op jit(solution)/shard_map/all_to_all | solution.py:184
  85.1 15.8 %all-to-all-start.2 = ((bf16[1024,2,256]{0,2,1:T(8,128)(2,1)}), bf16[1024,2,256]{0,2,1:T(8,128)(2,1)}, u32[]{:S(2)}, u32[]{:S(2)}) async-start(bf16[1024,2,256]{0,2,1:T(8,128)(2,1)} %bitcast.146), calls=%async_computation.2 | async-start | bytes 2097152 | tf_op jit(solution)/shard_map/all_to_all | solution.py:181
  91.8 14.4 %copy-start.12 = (f32[4]{0:T(128)S(1)}, f32[4]{0:T(128)}, u32[]{:S(2)}) copy-start(f32[4]{0:T(128)} %param.29) | copy-start | bytes 52
  100.9 15.0 %all-to-all-start.1 = ((bf16[1024,2,256]{0,2,1:T(8,128)(2,1)}), bf16[1024,2,256]{0,2,1:T(8,128)(2,1)}, u32[]{:S(2)}, u32[]{:S(2)}) async-start(bf16[1024,2,256]{0,2,1:T(8,128)(2,1)} %bitcast.142), calls=%async_computation.1 | async-start | bytes 2097152 | tf_op jit(solution)/shard_map/all_to_all | solution.py:171
  105.4 129.2 %all-gather.9.cloned.1.call-start = ((), (), s32[]{:S(2)}) async-start(), calls=%async_computation.10 | async-start | bytes 3145728 | tf_op jit(solution)/shard_map/all_gather | solution.py:224
  114.1 8.6 %copy-start.7 = (bf16[2,1024,256]{2,1,0:T(8,128)(2,1)S(1)}, bf16[2,1024,256]{2,1,0:T(8,128)(2,1)}, u32[]{:S(2)}) copy-start(bf16[2,1024,256]{2,1,0:T(8,128)(2,1)} %copy.87) | copy-start | bytes 3145732
  115.9 58.2 %all-to-all-start = ((bf16[2,1024,256]{2,1,0:T(8,128)(2,1)}), bf16[2,1024,256]{2,1,0:T(8,128)(2,1)}, u32[]{:S(2)}, u32[]{:S(2)}) async-start(bf16[2,1024,256]{2,1,0:T(8,128)(2,1)} %pad_maximum_fusion), calls=%async_computation | async-start | bytes 2097152 | tf_op jit(solution)/shard_map/all_to_all | solution.py:173
  122.6 4.4 %copy-start.1 = (bf16[1,256,2048]{2,1,0:T(8,128)(2,1)S(1)}, bf16[1,256,2048]{2,1,0:T(8,128)(2,1)}, u32[]{:S(2)}) copy-start(bf16[1,256,2048]{2,1,0:T(8,128)(2,1)} %all-gather.11.cloned.1.call-done) | copy-start | bytes 3145732
  125.1 6.1 %copy-start.3 = (bf16[2,1024,256]{2,1,0:T(8,128)(2,1)S(1)}, bf16[2,1024,256]{2,1,0:T(8,128)(2,1)}, u32[]{:S(2)}) copy-start(bf16[2,1024,256]{2,1,0:T(8,128)(2,1)} %copy.90) | copy-start | bytes 3145732
  143.1 3.6 %copy-start.10 = (f32[2,2,2,64,128]{4,3,0,2,1:T(8,128)S(1)}, f32[2,2,2,64,128]{4,3,0,2,1:T(8,128)}, u32[]{:S(2)}) copy-start(f32[2,2,2,64,128]{4,3,0,2,1:T(8,128)} %get-tuple-element.373) | copy-start | bytes 786436
  175.9 32.5 %copy-start.2 = (bf16[2,1024,256]{2,1,0:T(8,128)(2,1)S(1)}, bf16[2,1024,256]{2,1,0:T(8,128)(2,1)}, u32[]{:S(2)}) copy-start(bf16[2,1024,256]{2,1,0:T(8,128)(2,1)} %copy.80) | copy-start | bytes 3145732
  217.0 5.2 %copy-start.8 = (f32[2,128,2,128]{1,3,2,0:T(8,128)S(1)}, f32[2,128,2,128]{1,3,2,0:T(8,128)}, u32[]{:S(2)}) copy-start(f32[2,128,2,128]{1,3,2,0:T(8,128)} %copy.98) | copy-start | bytes 786436
  217.0 5.2 %copy-start.9 = (f32[2,128,2,128]{3,2,1,0:T(2,128)S(1)}, f32[2,128,2,128]{3,2,1,0:T(2,128)}, u32[]{:S(2)}) copy-start(f32[2,128,2,128]{3,2,1,0:T(2,128)} %get-tuple-element.522) | copy-start | bytes 786436
  217.8 8.9 %all-to-all-start.3 = ((bf16[2,128,256]{1,2,0:T(8,128)(2,1)}), bf16[2,128,256]{1,2,0:T(8,128)(2,1)S(1)}, u32[]{:S(2)}, u32[]{:S(2)}) async-start(bf16[2,128,256]{1,2,0:T(8,128)(2,1)} %bitcast.17), calls=%async_computation.3 | async-start | bytes 262144 | tf_op jit(solution)/shard_map/all_to_all | solution.py:219
  222.2 0.7 copy-start.11
  226.7 7.8 %all-to-all-start.7 = ((bf16[2,128,256]{1,2,0:T(8,128)(2,1)}), bf16[2,128,256]{1,2,0:T(8,128)(2,1)S(1)}, u32[]{:S(2)}, u32[]{:S(2)}) async-start(bf16[2,128,256]{1,2,0:T(8,128)(2,1)} %bitcast.38), calls=%async_computation.7 | async-start | bytes 262144 | tf_op jit(solution)/shard_map/all_to_all | solution.py:220
  230.1 34.5 %reduce-scatter.2.cloned.1.call-start = ((), (), s32[]{:S(2)}) async-start(), calls=%async_computation.11 | async-start | bytes 786432 | tf_op jit(solution)/shard_map/reduce_scatter | solution.py:227
Sparse Core Ops, SparseCore 0:
  11.3 31.6 all-gather.10
  44.5 45.7 all-gather.6
  107.8 44.8 all-gather.8
  237.6 27.0 reduce-scatter.1
